TPU v7x, 32 devices: a whole 2x2x4 slice. The times are simulated.
32 devices in a mesh: ep: 16 (over z, y, x), tp: 2 (over core).
Axes of the slice: x: 2, y: 2, z: 4, core: 2. Of those that a mesh axis runs over, the one named last changes fastest.
Arguments:
- tokens: bfloat16 [512, 1024], P('ep'), may hold values from -6 to 6
- norm_gain: float32 [1024], replicated, may hold values from 0.1 to 1.9
- routing: int32 [512, 4], P('ep'), may hold values from 0 to 15, all different within a row; in each aligned block of 32 rows (0 to 31, 32 to 63, ...) at most 16 rows name the same one
- route_logits: float32 [512, 4], P('ep'), may hold values from -6 to 6
- w_gate: bfloat16 [16, 1024, 1024], P('ep', None, 'tp'), may hold values from -0.1875 to 0.1875
- w_up: bfloat16 [16, 1024, 1024], P('ep', None, 'tp'), may hold values from -0.1875 to 0.1875
- w_down: bfloat16 [16, 1024, 1024], P('ep', None, 'tp'), may hold values from -0.1875 to 0.1875
Outputs:
- mixed: bfloat16 [512, 1024], P('ep', 'tp')
Inputs may be any that keep to these rules, and one draw needn't show every extreme that they name: `routing`: each row names 4 different experts; among the 32 tokens of one index of ep (aligned blocks of rows) no expert is named by more than 16 rows, and some block has an expert named by exactly 16.
All inputs are finite; a program needn't handle non-finite values.
Results may differ from a plain program's by a relative error of at most 0.0085.
Values may be sent and summed in bfloat16 or wider, within the bound.
A program may use at most 64 MiB of HBM per device.

v0:
```python
import jax
import jax.numpy as jnp
from jax import lax
from jax.sharding import PartitionSpec as P

CAP = 16


eps = 1e-05


def taken_in(share, axis, dim, step, start):
    def gathered(part):
        return lax.all_gather(part, axis, axis=dim, tiled=True)

    return step(start, jax.tree.map(gathered, share), jnp.int32(0))


def clamped(gate_part, up_part):
    limited = jnp.minimum(gate_part, 7.0)
    linear = jnp.clip(up_part, -7.0, 7.0)
    return limited * jax.nn.sigmoid(1.702 * limited) * (linear + 1.0)


def expert_rows(rows, w_gate, w_up, w_down):
    gate_part = jnp.dot(rows, w_gate[0], preferred_element_type=jnp.float32)
    up_part = jnp.dot(rows, w_up[0], preferred_element_type=jnp.float32)
    hidden = clamped(gate_part, up_part).astype(jnp.bfloat16)
    down_local = w_down[0]
    empty = jnp.zeros((rows.shape[0], down_local.shape[1]), jnp.float32)

    def add_rows(total, piece, start):
        weights = lax.dynamic_slice_in_dim(down_local, start, piece.shape[1], 0)
        return total + jnp.dot(piece, weights, preferred_element_type=jnp.float32)

    summed = taken_in(hidden, "tp", 1, add_rows, empty)
    return summed.astype(jnp.bfloat16)


def shards(tokens, norm_gain, routing, route_logits, w_gate, w_up, w_down):
    as_float = tokens.astype(jnp.float32)
    scaled = as_float * lax.rsqrt(jnp.mean(as_float * as_float, axis=-1, keepdims=True) + eps)
    normed = (scaled * norm_gain).astype(jnp.bfloat16)
    gate_probs = jax.nn.softmax(route_logits, axis=-1)
    tok_dev = tokens.shape[0]
    topk = routing.shape[1]
    width = tokens.shape[1]
    n_ep = lax.axis_size("ep")
    assigns = tok_dev * topk
    flat_e = routing.reshape(-1)
    onehot = (flat_e[:, None] == jnp.arange(n_ep, dtype=jnp.int32)[None, :]).astype(jnp.int32)
    slot_rank = jnp.sum((jnp.cumsum(onehot, axis=0) - onehot) * onehot, axis=1).astype(jnp.int32)
    slot_index = flat_e * CAP + slot_rank
    flat_tok = jnp.arange(assigns, dtype=jnp.int32) // topk
    outbound = jnp.zeros((n_ep * CAP, width), jnp.bfloat16).at[slot_index].set(normed[flat_tok])
    arrived = lax.all_to_all(
        outbound.reshape(n_ep, CAP, width), "ep", split_axis=0, concat_axis=0, tiled=True
    )
    expert_out = expert_rows(arrived.reshape(n_ep * CAP, width), w_gate, w_up, w_down)
    half_width = expert_out.shape[1]
    returned_rows = lax.all_to_all(
        expert_out.reshape(n_ep, CAP, half_width), "ep", split_axis=0, concat_axis=0, tiled=True
    )
    returned_rows = returned_rows.reshape(n_ep * CAP, half_width)
    picked = returned_rows[slot_index].astype(jnp.float32) * gate_probs.reshape(-1)[:, None]
    mixed = jnp.sum(picked.reshape(tok_dev, topk, half_width), axis=1).astype(jnp.bfloat16)
    return mixed


def solution(mesh):
    return jax.shard_map(
        shards,
        mesh=mesh,
        in_specs=(
            P("ep", None),
            P(),
            P("ep", None),
            P("ep", None),
            P("ep", None, "tp"),
            P("ep", None, "tp"),
            P("ep", None, "tp"),
        ),
        out_specs=P("ep", "tp"),
        check_vma=False,
    )
```

profile of v0, /device:TPU:0, one launch (start us, length us, event | category | flops | bytes accessed | tf_op | source)
XLA Modules:
  0.0 50.0 jit_solution(11041559288213418174)
XLA Ops:
  0.0 0.9 %copy.12 = s32[32,4]{1,0:T(8,128)S(1)} copy(s32[32,4]{0,1:T(4,128)} %param.9) | data formatting | bytes 1024 | tf_op args[2]
  0.9 0.1 eq.15
  1.0 0.1 fusion.12
  1.1 0.2 reduce_window_sum.11
  1.3 0.2 select_reduce_fusion
  1.4 0.1 copy.11
  1.5 0.1 mul.61
  1.6 0.5 copy-done.2
  2.1 0.1 fusion.9
  2.3 0.6 %copy-done.5 = f32[1024]{0:T(1024)S(1)} copy-done((f32[1024]{0:T(1024)S(1)}, f32[1024]{0:T(1024)}, u32[]{:S(2)}) %copy-start.5) | copy-done | bytes 4120
  2.9 0.1 fusion.11
  3.0 2.2 %scatter_custom_fusion = bf16[256,1024]{1,0:T(8,128)(2,1)S(1)} fusion(s32[128]{0:T(128)S(1)} %fusion.16, bf16[32,1024]{1,0:T(8,128)(2,1)S(1)} %fusion.11, s32[1024]{0:T(1024)S(1)} %pad_clamp_fusion.1, bf16[]{:T(256)} %constant.17.clone.1), kind=kCustom, calls=%fused_computation.12 | custom fusion | bytes 524290 | tf_op jit(solution)/shard_map/scatter | solution.py:55
  5.2 23.3 %all_to_all.10 = bf16[16,16,1024]{2,1,0:T(8,128)(2,1)S(1)} all-to-all(bf16[16,16,1024]{2,1,0:T(8,128)(2,1)S(1)} %bitcast.25), channel_id=1, replica_groups=mesh['ep'=16,'tp'=2] {'ep'}, dimensions={0} | all-to-all | bytes 1048576 | tf_op jit(solution)/shard_map/all_to_all | solution.py:56
  28.5 0.4 convolution_minimum_fusion
  28.9 0.8 %copy-done.6 = bf16[1,1024,512]{2,1,0:T(8,128)(2,1)S(1)} copy-done((bf16[1,1024,512]{2,1,0:T(8,128)(2,1)S(1)}, bf16[1,1024,512]{2,1,0:T(8,128)(2,1)}, u32[]{:S(2)}) %copy-start.6) | copy-done | bytes 1048600
  29.7 0.5 fusion.2
  30.2 2.2 %all_gather.3 = bf16[256,1024]{1,0:T(8,128)(2,1)S(1)} all-gather(bf16[256,512]{1,0:T(8,128)(2,1)S(1)} %fusion.2), channel_id=1, replica_groups=mesh['ep'=16,'tp'=2] {'tp'}, dimensions={1}, use_global_device_ids=true | all-gather | bytes 786432 | tf_op jit(solution)/shard_map/all_gather | solution.py:14
  32.4 1.1 %convolution_convert_fusion = bf16[256,512]{1,0:T(8,128)(2,1)} fusion(bf16[256,1024]{1,0:T(8,128)(2,1)S(1)} %all_gather.3, bf16[1,1024,512]{2,1,0:T(8,128)(2,1)S(1)} %copy-done.1), kind=kOutput, calls=%fused_computation.8 | convolution fusion | flops 268566528 | bytes 1835008 | tf_op jit(solution)/shard_map/dot_general | solution.py:34
  33.6 4.0 %all-to-all-start.1 = ((bf16[16,16,512]{2,1,0:T(8,128)(2,1)}), bf16[16,16,512]{2,1,0:T(8,128)(2,1)S(1)}, u32[]{:S(2)}, u32[]{:S(2)}) async-start(bf16[16,16,512]{2,1,0:T(8,128)(2,1)} %bitcast.8), calls=%async_computation.1 | async-start | bytes 524288 | tf_op jit(solution)/shard_map/all_to_all | solution.py:61
  37.6 0.1 copy.13
  37.7 10.5 %all-to-all-done.1 = bf16[16,16,512]{2,1,0:T(8,128)(2,1)S(1)} async-done(((bf16[16,16,512]{2,1,0:T(8,128)(2,1)}), bf16[16,16,512]{2,1,0:T(8,128)(2,1)S(1)}, u32[]{:S(2)}, u32[]{:S(2)}) %all-to-all-start.1) | async-done | bytes 262176 | tf_op jit(solution)/shard_map/all_to_all | solution.py:61
  48.2 0.8 %gather_fusion = bf16[128,512]{1,0:T(8,128)(2,1)S(1)} fusion(bf16[256,512]{1,0:T(8,128)(2,1)S(1)} %bitcast.24, s32[1024]{0:T(1024)S(1)} %pad_clamp_fusion), kind=kCustom, calls=%fused_computation.1 | custom fusion | bytes 262656 | tf_op jit(solution)/shard_map/gather | solution.py:65
  49.0 0.1 reshape.110
  49.1 0.8 %multiply_reduce_fusion = bf16[32,512]{1,0:T(8,128)(2,1)} fusion(f32[32,4,512]{2,1,0:T(4,128)S(1)} %reshape.110, f32[32,4]{1,0:T(8,128)S(1)} %copy.13), kind=kLoop, calls=%fused_computation.14 | loop fusion | flops 114688 | bytes 295424 | tf_op jit(solution)/shard_map/reduce_sum | solution.py:66
  (20 shorter events, 0.1 us)
Async XLA Ops:
  0.0 28.5 %copy-start = (bf16[1,1024,512]{2,1,0:T(8,128)(2,1)S(1)}, bf16[1,1024,512]{2,1,0:T(8,128)(2,1)}, u32[]{:S(2)}) copy-start(bf16[1,1024,512]{2,1,0:T(8,128)(2,1)} %param.11) | copy-start | bytes 3145732
  0.0 0.9 %copy-start.4 = (s32[32,4]{0,1:T(4,128)S(1)}, s32[32,4]{0,1:T(4,128)}, u32[]{:S(2)}) copy-start(s32[32,4]{0,1:T(4,128)} %param.9) | copy-start | bytes 1540
  1.3 0.8 %copy-start.2 = (bf16[32,1024]{1,0:T(8,128)(2,1)S(1)}, bf16[32,1024]{1,0:T(8,128)(2,1)}, u32[]{:S(2)}) copy-start(bf16[32,1024]{1,0:T(8,128)(2,1)} %param.7) | copy-start | bytes 196612
  2.2 0.7 %copy-start.5 = (f32[1024]{0:T(1024)S(1)}, f32[1024]{0:T(1024)}, u32[]{:S(2)}) copy-start(f32[1024]{0:T(1024)} %param.8) | copy-start | bytes 12292
  28.5 1.2 %copy-start.6 = (bf16[1,1024,512]{2,1,0:T(8,128)(2,1)S(1)}, bf16[1,1024,512]{2,1,0:T(8,128)(2,1)}, u32[]{:S(2)}) copy-start(bf16[1,1024,512]{2,1,0:T(8,128)(2,1)} %param.12) | copy-start | bytes 3145732
  29.7 2.7 %copy-start.1 = (bf16[1,1024,512]{2,1,0:T(8,128)(2,1)S(1)}, bf16[1,1024,512]{2,1,0:T(8,128)(2,1)}, u32[]{:S(2)}) copy-start(bf16[1,1024,512]{2,1,0:T(8,128)(2,1)} %param.13) | copy-start | bytes 3145732
  33.6 4.0 %copy-start.3 = (f32[32,4]{0,1:T(4,128)S(1)}, f32[32,4]{0,1:T(4,128)}, u32[]{:S(2)}) copy-start(f32[32,4]{0,1:T(4,128)} %param.10) | copy-start | bytes 1540
  33.6 14.6 %all-to-all-start.1 = ((bf16[16,16,512]{2,1,0:T(8,128)(2,1)}), bf16[16,16,512]{2,1,0:T(8,128)(2,1)S(1)}, u32[]{:S(2)}, u32[]{:S(2)}) async-start(bf16[16,16,512]{2,1,0:T(8,128)(2,1)} %bitcast.8), calls=%async_computation.1 | async-start | bytes 524288 | tf_op jit(solution)/shard_map/all_to_all | solution.py:61
where the time goes:
time: 50.4 us; the launch traced here: 50 us
  blocking collectives  25.5 us (51%)
  waiting for transfers between devices  10.5 us (21%)
  local copies, waits for them, and re-layouts  6.3 us (12%)
  starting transfers between devices  3.95 us (8%)
  matrix products  2.06 us (4%)
  other arithmetic  1.58 us (3%)
    all_to_all x1, blocking collectives, shards(): lax.all_to_all(outbound.reshape(n_ep, CAP, width), 'ep', split_axis=0, co...  23.3 us
    all_to_all x1, waiting for transfers between devices, shards(): lax.all_to_all(expert_out.reshape(n_ep, CAP, half_width), 'ep', split_axi...  10.5 us
    all_to_all x1, starting transfers between devices, shards(): lax.all_to_all(expert_out.reshape(n_ep, CAP, half_width), 'ep', split_axi...  3.95 us
    unnamed x15, local copies, waits for them, and re-layouts  2.77 us
    scatter x1, local copies, waits for them, and re-layouts, shards(): jnp.zeros((n_ep * CAP, width), jnp.bfloat16).at[slot_index]  2.2 us
    all_gather x1, blocking collectives, gathered(): return lax.all_gather(part, axis, axis=dim, tiled=True)  2.19 us
    dot_general x1, matrix products, add_rows(): return total + jnp.dot(piece, weights, preferred_element_type=jnp.float32)  1.15 us
  transfers between devices with their start and end apart: 1, of which 1 were waited for; matrix products, arithmetic and copies ran while one was open for 0% of the time, Pallas kernels for 0%

commit v1 on v0

v1 whole, which is shorter than its diff:
```python
import functools

import jax
import jax.numpy as jnp
from jax import lax
from jax.experimental import pallas as pl
from jax.experimental.pallas import tpu as pltpu
from jax.sharding import PartitionSpec as P

CAP = 16
MESH = pl.DeviceIdType.MESH

eps = 1e-05


def each(count, step):
    if count <= 16:
        for k in range(count):
            step(k)
    else:
        lax.fori_loop(0, count, lambda k, carry: (step(k), carry)[1], 0)


def mm(a, b):
    return jnp.dot(a, b, preferred_element_type=jnp.float32)


def kernel(n, x_ref, gain_ref, route_ref, logit_ref, wg_hbm, wu_hbm, wd_hbm, out_ref,
           wg, wu, wd, outb, arr, gp, up, hid, eo, ret,
           wsem, dsend, drecv, fsend, frecv, hsend, hrecv, rsend, rrecv):
    me, c = lax.axis_index("ep"), lax.axis_index("tp")
    other = 1 - c
    tok, width = x_ref.shape
    topk = route_ref.shape[1]
    half = outb.shape[2]
    fh = hid.shape[2]
    dh = eo.shape[2]
    rows = n * CAP
    step_rows = min(rows, 256)

    barrier = pltpu.get_barrier_semaphore()
    pl.semaphore_signal(barrier, inc=1, device_id=(me, other), device_id_type=MESH)

    def greet(k):
        pl.semaphore_signal(barrier, inc=1, device_id=(lax.rem(me + k + 1, n), c), device_id_type=MESH)

    each(n - 1, greet)

    loads = [pltpu.make_async_copy(src.at[0], dst, wsem.at[i])
             for i, (src, dst) in enumerate(((wg_hbm, wg), (wu_hbm, wu), (wd_hbm, wd)))]
    for load in loads:
        load.start()

    lane = lax.broadcasted_iota(jnp.int32, (tok, rows), 1)
    expert, slot = lax.div(lane, CAP), lax.rem(lane, CAP)
    route = route_ref[...]
    logits = logit_ref[...]
    raised = jnp.exp(logits - jnp.max(logits, axis=1, keepdims=True))
    probs = raised / jnp.sum(raised, axis=1, keepdims=True)
    named = jnp.zeros((tok, rows), jnp.float32)
    weight = jnp.zeros((tok, rows), jnp.float32)
    for k in range(topk):
        hit = route[:, k:k + 1] == expert
        named = jnp.where(hit, 1.0, named)
        weight = jnp.where(hit, probs[:, k:k + 1], weight)
    earlier = (lax.broadcasted_iota(jnp.int32, (tok, tok), 1)
               < lax.broadcasted_iota(jnp.int32, (tok, tok), 0))
    earlier = jnp.where(earlier, 1.0, 0.0).astype(jnp.bfloat16)
    rank = mm(earlier, named.astype(jnp.bfloat16))
    here = rank == slot.astype(jnp.float32)
    place = jnp.where(here, named, 0.0).astype(jnp.bfloat16)
    weight = jnp.where(here, weight, 0.0)

    x = x_ref[...].astype(jnp.float32)
    inv = lax.rsqrt(jnp.mean(x * x, axis=1, keepdims=True) + eps)
    own_cols = pl.ds(pl.multiple_of(c * half, half), half)
    mine = ((x_ref[:, own_cols].astype(jnp.float32) * inv) * gain_ref[:, own_cols]).astype(jnp.bfloat16)
    outb[...] = lax.dot_general(place, mine, (((0,), (0,)), ((), ())),
                                preferred_element_type=jnp.float32).astype(jnp.bfloat16).reshape(n, CAP, half)
    arr[c, me] = outb[me]

    pl.semaphore_wait(barrier, n)

    def forward(source):
        pltpu.make_async_remote_copy(
            arr.at[c, source], arr.at[c, source], fsend, frecv,
            device_id=(me, other), device_id_type=MESH).start()

    def send(k):
        to = lax.rem(me + k + 1, n)
        pltpu.make_async_remote_copy(
            outb.at[to], arr.at[c, me], dsend, drecv.at[me],
            device_id=(to, c), device_id_type=MESH).start()

    each(n - 1, send)
    forward(me)

    def pass_on(k):
        source = lax.rem(me + n - k - 1, n)
        pltpu.make_async_remote_copy(
            outb.at[source], arr.at[c, source], dsend, drecv.at[source],
            device_id=(source, c), device_id_type=MESH).wait_recv()
        forward(source)

    each(n - 1, pass_on)

    own_in = pl.ds(pl.multiple_of(c * half, half), half)
    other_in = pl.ds(pl.multiple_of(other * half, half), half)
    own_hid = pl.ds(pl.multiple_of(c * fh, fh), fh)
    other_hid = pl.ds(pl.multiple_of(other * fh, fh), fh)
    per = step_rows // CAP
    loads[0].wait()
    loads[1].wait()

    def first_half(i):
        rs = pl.ds(i * step_rows, step_rows)
        a = arr[c, pl.ds(i * per, per)].reshape(step_rows, half)
        gp[rs] = mm(a, wg[own_in])
        up[rs] = mm(a, wu[own_in])

    each(rows // step_rows, first_half)
    pltpu.make_async_copy(arr.at[other], arr.at[other], frecv).wait()

    def second_half(i):
        rs = pl.ds(i * step_rows, step_rows)
        a = arr[other, pl.ds(i * per, per)].reshape(step_rows, half)
        g = jnp.minimum(gp[rs] + mm(a, wg[other_in]), 7.0)
        l = jnp.clip(up[rs] + mm(a, wu[other_in]), -7.0, 7.0)
        hid[c, rs] = (g * jax.nn.sigmoid(1.702 * g) * (l + 1.0)).astype(jnp.bfloat16)

    each(rows // step_rows, second_half)
    swap = pltpu.make_async_remote_copy(
        hid.at[c], hid.at[c], hsend, hrecv, device_id=(me, other), device_id_type=MESH)
    swap.start()
    loads[2].wait()

    def first_down(i):
        rs = pl.ds(i * step_rows, step_rows)
        gp[rs] = mm(hid[c, rs], wd[own_hid])

    each(rows // step_rows, first_down)
    pltpu.make_async_copy(hid.at[other], hid.at[other], hrecv).wait()

    def second_down(i):
        rs = pl.ds(i * step_rows, step_rows)
        total = gp[rs] + mm(hid[other, rs], wd[other_hid])
        eo[pl.ds(i * per, per)] = total.astype(jnp.bfloat16).reshape(per, CAP, dh)

    each(rows // step_rows, second_down)

    def give_back(k):
        to = lax.rem(me + k + 1, n)
        pltpu.make_async_remote_copy(
            eo.at[to], ret.at[me], rsend, rrecv,
            device_id=(to, c), device_id_type=MESH).start()

    each(n - 1, give_back)
    ret[me] = eo[me]
    high = weight.astype(jnp.bfloat16)
    low = (weight - high.astype(jnp.float32)).astype(jnp.bfloat16)
    others = pl.ds(0, n - 1)
    pltpu.make_async_copy(ret.at[others], ret.at[others], rrecv).wait()
    back = ret[...].reshape(rows, dh)
    out_ref[...] = (mm(high, back) + mm(low, back)).astype(out_ref.dtype)

    pltpu.make_async_copy(outb.at[others], outb.at[others], dsend).wait()
    pltpu.make_async_copy(arr.at[c], arr.at[c], fsend).wait()
    swap.wait_send()
    pltpu.make_async_copy(eo.at[others], eo.at[others], rsend).wait()


def shards(tokens, norm_gain, routing, route_logits, w_gate, w_up, w_down):
    n = lax.axis_size("ep")
    tok, width = tokens.shape
    half = width // lax.axis_size("tp")
    fh = w_gate.shape[2]
    dh = w_down.shape[2]
    rows = n * CAP
    vmem = pl.BlockSpec(memory_space=pltpu.VMEM)
    hbm = pl.BlockSpec(memory_space=pl.ANY)
    bf16, f32 = jnp.bfloat16, jnp.float32
    dma = pltpu.SemaphoreType.DMA
    return pl.pallas_call(
        functools.partial(kernel, n),
        out_shape=jax.ShapeDtypeStruct((tok, dh), bf16),
        in_specs=[vmem] * 4 + [hbm] * 3,
        out_specs=vmem,
        scratch_shapes=[
            pltpu.VMEM(w_gate.shape[1:], bf16),
            pltpu.VMEM(w_up.shape[1:], bf16),
            pltpu.VMEM(w_down.shape[1:], bf16),
            pltpu.VMEM((n, CAP, half), bf16),
            pltpu.VMEM((2, n, CAP, half), bf16),
            pltpu.VMEM((rows, fh), f32),
            pltpu.VMEM((rows, fh), f32),
            pltpu.VMEM((2, rows, fh), bf16),
            pltpu.VMEM((n, CAP, dh), bf16),
            pltpu.VMEM((n, CAP, dh), bf16),
            dma((3,)),
            dma,
            dma((n,)),
            dma,
            dma,
            dma,
            dma,
            dma,
            dma,
        ],
        compiler_params=pltpu.CompilerParams(
            collective_id=0, has_side_effects=True, vmem_limit_bytes=60 * 1024 * 1024),
    )(tokens, norm_gain.reshape(1, width), routing, route_logits, w_gate, w_up, w_down)


def solution(mesh):
    return jax.shard_map(
        shards,
        mesh=mesh,
        in_specs=(
            P("ep", None),
            P(),
            P("ep", None),
            P("ep", None),
            P("ep", None, "tp"),
            P("ep", None, "tp"),
            P("ep", None, "tp"),
        ),
        out_specs=P("ep", "tp"),
        check_vma=False,
    )
```

time: 50.4 us -> 28.8 us (0.57)
  blocking collectives: 25.5 us -> 0 us
  Pallas kernels: 0 us -> 25.1 us
  waiting for transfers between devices: 10.5 us -> 0 us
  starting transfers between devices: 3.95 us -> 0 us
  local copies, waits for them, and re-layouts: 6.3 us -> 3.44 us
  matrix products: 2.06 us -> 0 us
  other arithmetic: 1.58 us -> 0 us
    pallas_call x0 -> x1, Pallas kernels: none -> 25.1 us  [shards(): pl.pallas_call(functools.partial(kernel, n), out_shape=jax.ShapeDtypeStru...]
    all_to_all x1 -> x0, blocking collectives: 23.3 us -> none  [shards(): lax.all_to_all(outbound.reshape(n_ep, CAP, width), 'ep', split_axis=0, co...]
    all_to_all x1 -> x0, waiting for transfers between devices: 10.5 us -> none  [shards(): lax.all_to_all(expert_out.reshape(n_ep, CAP, half_width), 'ep', split_axi...]
    all_to_all x1 -> x0, starting transfers between devices: 3.95 us -> none  [shards(): lax.all_to_all(expert_out.reshape(n_ep, CAP, half_width), 'ep', split_axi...]
    scatter x1 -> x0, local copies, waits for them, and re-layouts: 2.2 us -> none  [shards(): jnp.zeros((n_ep * CAP, width), jnp.bfloat16).at[slot_index]]
    all_gather x1 -> x0, blocking collectives: 2.19 us -> none  [gathered(): return lax.all_gather(part, axis, axis=dim, tiled=True)]
    dot_general x3 -> x0, matrix products: 2.06 us -> none  [the longest x1 1.15 us: add_rows(): return total + jnp.dot(piece, weights, preferred_element_type=jnp.float32)]
    reduce_sum x4 -> x0, other arithmetic: 1.17 us -> none  [the longest x1 0.85 us: shards(): jnp.sum(picked.reshape(tok_dev, topk, half_width), axis=1)]
  transfers between devices with their start and end apart: 1 -> 0, of which waited for: 1 -> 0; matrix products, arithmetic and copies ran while one was open for 0% -> 0% of each run, Pallas kernels for 0% -> 0%
where the time goes in v1:
time: 28.8 us; the launch traced here: 28.6 us
  Pallas kernels  25.1 us (87%)
  local copies, waits for them, and re-layouts  3.44 us (12%)
    pallas_call x1, Pallas kernels, shards(): pl.pallas_call(functools.partial(kernel, n), out_shape=jax.ShapeDtypeStru...  25.1 us
    unnamed x5, local copies, waits for them, and re-layouts  3.44 us

profile of v1, /device:TPU:0, one launch (start us, length us, event | category | flops | bytes accessed | tf_op | source)
XLA Modules:
  0.0 28.6 jit_solution(8876549651403763190)
XLA Ops:
  0.0 0.0 copy-start
  0.0 1.4 %copy.8.route_ref = s32[32,4]{1,0:T(8,128)} copy(s32[32,4]{0,1:T(4,128)} %param.9) | data formatting | bytes 1024 | tf_op args[2]
  1.4 0.0 copy-done
  1.4 0.7 %copy.9.logit_ref = f32[32,4]{1,0:T(8,128)} copy(f32[32,4]{0,1:T(4,128)S(1)} %copy-done) | data formatting | bytes 1024 | tf_op args[3]
  2.1 25.1 %shard_map.73 = bf16[32,512]{1,0:T(8,128)(2,1)} custom-call(bf16[32,1024]{1,0:T(8,128)(2,1)} %x_ref.1, f32[1,1024]{1,0:T(1,128)} %bitcast.1, s32[32,4]{1,0:T(8,128)} %copy.8.route_ref, f32[32,4]{1,0:T(8,128)} %copy.9.logit_ref, bf16[1,1024,512]{2,1,0:T(8,128)(2,1)} %wg_hbm.1, bf16[1,1024,512]{2,1,0:T(8,128)(2,1)} %wu_hbm.1, bf16[1,1024,512]{2,1,0:T(8,128)(2,1)} %wd_hbm.1), custom_call_target="tpu_custom_call" | custom-call | tf_op jit(solution)/shard_map/pallas_call | solution.py:183
  27.2 1.4 %copy.11 = bf16[32,512]{1,0:T(8,128)(2,1)} copy(bf16[32,512]{1,0:T(8,128)(2,1)} %shard_map.73) | data formatting | bytes 65536
Async XLA Ops:
  0.0 1.4 %copy-start = (f32[32,4]{0,1:T(4,128)S(1)}, f32[32,4]{0,1:T(4,128)}, u32[]{:S(2)}) copy-start(f32[32,4]{0,1:T(4,128)} %param.10) | copy-start | bytes 1540

commit v2 on v1

--- a/solution.py
+++ b/solution.py
@@ -36,7 +36,7 @@
     fh = hid.shape[2]
     dh = eo.shape[2]
     rows = n * CAP
-    step_rows = min(rows, 256)
+    step_rows = min(rows // 2, 256)
 
     barrier = pltpu.get_barrier_semaphore()
     pl.semaphore_signal(barrier, inc=1, device_id=(me, other), device_id_type=MESH)
@@ -81,80 +81,109 @@
 
     pl.semaphore_wait(barrier, n)
 
-    def forward(source):
-        pltpu.make_async_remote_copy(
-            arr.at[c, source], arr.at[c, source], fsend, frecv,
+    group = n // 2
+    own_base = lax.div(me, group) * group
+    far_base = (n - group) - own_base
+    at = me - own_base
+
+    def forward(source, part):
+        pltpu.make_async_remote_copy(
+            arr.at[c, source], arr.at[c, source], fsend, frecv.at[part],
             device_id=(me, other), device_id_type=MESH).start()
 
-    def send(k):
-        to = lax.rem(me + k + 1, n)
+    def near(k):
+        return own_base + lax.rem(at + k + 1, group)
+
+    def far(k):
+        return far_base + lax.rem(at + k, group)
+
+    def send(to):
         pltpu.make_async_remote_copy(
             outb.at[to], arr.at[c, me], dsend, drecv.at[me],
             device_id=(to, c), device_id_type=MESH).start()
 
-    each(n - 1, send)
-    forward(me)
-
-    def pass_on(k):
-        source = lax.rem(me + n - k - 1, n)
+    def pass_on(source, part):
         pltpu.make_async_remote_copy(
             outb.at[source], arr.at[c, source], dsend, drecv.at[source],
             device_id=(source, c), device_id_type=MESH).wait_recv()
-        forward(source)
-
-    each(n - 1, pass_on)
+        forward(source, part)
+
+    def give_back(to):
+        pltpu.make_async_remote_copy(
+            eo.at[to], ret.at[me], rsend, rrecv,
+            device_id=(to, c), device_id_type=MESH).start()
+
+    each(group, lambda k: send(far(k)))
+    each(group - 1, lambda k: send(near(k)))
+    forward(me, 0)
 
     own_in = pl.ds(pl.multiple_of(c * half, half), half)
     other_in = pl.ds(pl.multiple_of(other * half, half), half)
     own_hid = pl.ds(pl.multiple_of(c * fh, fh), fh)
     other_hid = pl.ds(pl.multiple_of(other * fh, fh), fh)
     per = step_rows // CAP
+    steps = group * CAP // step_rows
+
+    def run_experts(part, base):
+        whole = pl.ds(base, group)
+        first_row = pl.multiple_of(base * CAP, group * CAP)
+        whole_rows = pl.ds(first_row, group * CAP)
+
+        def rows_at(i):
+            return pl.ds(pl.multiple_of(first_row + i * step_rows, step_rows), step_rows)
+
+        def blocks_at(i):
+            return pl.ds(base + i * per, per)
+
+        def first_half(i):
+            rs = rows_at(i)
+            a = arr[c, blocks_at(i)].reshape(step_rows, half)
+            gp[rs] = mm(a, wg[own_in])
+            up[rs] = mm(a, wu[own_in])
+
+        each(steps, first_half)
+        waited = arr.at[other, whole]
+        pltpu.make_async_copy(waited, waited, frecv.at[part]).wait()
+
+        def second_half(i):
+            rs = rows_at(i)
+            a = arr[other, blocks_at(i)].reshape(step_rows, half)
+            g = jnp.minimum(gp[rs] + mm(a, wg[other_in]), 7.0)
+            l = jnp.clip(up[rs] + mm(a, wu[other_in]), -7.0, 7.0)
+            hid[c, rs] = (g * jax.nn.sigmoid(1.702 * g) * (l + 1.0)).astype(jnp.bfloat16)
+
+        each(steps, second_half)
+        swap = pltpu.make_async_remote_copy(
+            hid.at[c, whole_rows], hid.at[c, whole_rows], hsend.at[part], hrecv.at[part],
+            device_id=(me, other), device_id_type=MESH)
+        swap.start()
+        if part == 0:
+            loads[2].wait()
+
+        def first_down(i):
+            rs = rows_at(i)
+            gp[rs] = mm(hid[c, rs], wd[own_hid])
+
+        each(steps, first_down)
+        swapped = hid.at[other, whole_rows]
+        pltpu.make_async_copy(swapped, swapped, hrecv.at[part]).wait()
+
+        def second_down(i):
+            rs = rows_at(i)
+            total = gp[rs] + mm(hid[other, rs], wd[other_hid])
+            eo[blocks_at(i)] = total.astype(jnp.bfloat16).reshape(per, CAP, dh)
+
+        each(steps, second_down)
+        return swap
+
+    each(group - 1, lambda k: pass_on(near(group - 2 - k), 0))
     loads[0].wait()
     loads[1].wait()
-
-    def first_half(i):
-        rs = pl.ds(i * step_rows, step_rows)
-        a = arr[c, pl.ds(i * per, per)].reshape(step_rows, half)
-        gp[rs] = mm(a, wg[own_in])
-        up[rs] = mm(a, wu[own_in])
-
-    each(rows // step_rows, first_half)
-    pltpu.make_async_copy(arr.at[other], arr.at[other], frecv).wait()
-
-    def second_half(i):
-        rs = pl.ds(i * step_rows, step_rows)
-        a = arr[other, pl.ds(i * per, per)].reshape(step_rows, half)
-        g = jnp.minimum(gp[rs] + mm(a, wg[other_in]), 7.0)
-        l = jnp.clip(up[rs] + mm(a, wu[other_in]), -7.0, 7.0)
-        hid[c, rs] = (g * jax.nn.sigmoid(1.702 * g) * (l + 1.0)).astype(jnp.bfloat16)
-
-    each(rows // step_rows, second_half)
-    swap = pltpu.make_async_remote_copy(
-        hid.at[c], hid.at[c], hsend, hrecv, device_id=(me, other), device_id_type=MESH)
-    swap.start()
-    loads[2].wait()
-
-    def first_down(i):
-        rs = pl.ds(i * step_rows, step_rows)
-        gp[rs] = mm(hid[c, rs], wd[own_hid])
-
-    each(rows // step_rows, first_down)
-    pltpu.make_async_copy(hid.at[other], hid.at[other], hrecv).wait()
-
-    def second_down(i):
-        rs = pl.ds(i * step_rows, step_rows)
-        total = gp[rs] + mm(hid[other, rs], wd[other_hid])
-        eo[pl.ds(i * per, per)] = total.astype(jnp.bfloat16).reshape(per, CAP, dh)
-
-    each(rows // step_rows, second_down)
-
-    def give_back(k):
-        to = lax.rem(me + k + 1, n)
-        pltpu.make_async_remote_copy(
-            eo.at[to], ret.at[me], rsend, rrecv,
-            device_id=(to, c), device_id_type=MESH).start()
-
-    each(n - 1, give_back)
+    swap_near = run_experts(0, own_base)
+    each(group - 1, lambda k: give_back(near(k)))
+    each(group, lambda k: pass_on(far(k), 1))
+    swap_far = run_experts(1, far_base)
+    each(group, lambda k: give_back(far(k)))
     ret[me] = eo[me]
     high = weight.astype(jnp.bfloat16)
     low = (weight - high.astype(jnp.float32)).astype(jnp.bfloat16)
@@ -165,7 +194,8 @@
 
     pltpu.make_async_copy(outb.at[others], outb.at[others], dsend).wait()
     pltpu.make_async_copy(arr.at[c], arr.at[c], fsend).wait()
-    swap.wait_send()
+    swap_near.wait_send()
+    swap_far.wait_send()
     pltpu.make_async_copy(eo.at[others], eo.at[others], rsend).wait()
 
 
@@ -200,9 +230,9 @@
             dma,
             dma((n,)),
             dma,
-            dma,
-            dma,
-            dma,
+            dma((2,)),
+            dma((2,)),
+            dma((2,)),
             dma,
             dma,
         ],

time: 28.8 us -> 30.5 us (1.059)
  Pallas kernels: 25.1 us -> 26.7 us
    pallas_call x1, Pallas kernels: 25.1 us -> 26.7 us  [shards(): pl.pallas_call(functools.partial(kernel, n), out_shape=jax.ShapeDtypeStru...]
where the time goes in v2:
time: 30.5 us; the launch traced here: 30.1 us
  Pallas kernels  26.7 us (88%)
  local copies, waits for them, and re-layouts  3.44 us (11%)
    pallas_call x1, Pallas kernels, shards(): pl.pallas_call(functools.partial(kernel, n), out_shape=jax.ShapeDtypeStru...  26.7 us
    unnamed x5, local copies, waits for them, and re-layouts  3.44 us

profile of v2, /device:TPU:0, one launch (start us, length us, event | category | flops | bytes accessed | tf_op | source)
XLA Modules:
  0.0 30.1 jit_solution(17331076832270224367)
XLA Ops:
  0.0 0.0 copy-start
  0.0 1.4 %copy.8.route_ref = s32[32,4]{1,0:T(8,128)} copy(s32[32,4]{0,1:T(4,128)} %param.9) | data formatting | bytes 1024 | tf_op args[2]
  1.4 0.0 copy-done
  1.4 0.7 %copy.9.logit_ref = f32[32,4]{1,0:T(8,128)} copy(f32[32,4]{0,1:T(4,128)S(1)} %copy-done) | data formatting | bytes 1024 | tf_op args[3]
  2.1 26.7 %shard_map.73 = bf16[32,512]{1,0:T(8,128)(2,1)} custom-call(bf16[32,1024]{1,0:T(8,128)(2,1)} %x_ref.1, f32[1,1024]{1,0:T(1,128)} %bitcast.1, s32[32,4]{1,0:T(8,128)} %copy.8.route_ref, f32[32,4]{1,0:T(8,128)} %copy.9.logit_ref, bf16[1,1024,512]{2,1,0:T(8,128)(2,1)} %wg_hbm.1, bf16[1,1024,512]{2,1,0:T(8,128)(2,1)} %wu_hbm.1, bf16[1,1024,512]{2,1,0:T(8,128)(2,1)} %wd_hbm.1), custom_call_target="tpu_custom_call" | custom-call | tf_op jit(solution)/shard_map/pallas_call | solution.py:213
  28.8 1.4 %copy.11 = bf16[32,512]{1,0:T(8,128)(2,1)} copy(bf16[32,512]{1,0:T(8,128)(2,1)} %shard_map.73) | data formatting | bytes 65536
Async XLA Ops:
  0.0 1.4 %copy-start = (f32[32,4]{0,1:T(4,128)S(1)}, f32[32,4]{0,1:T(4,128)}, u32[]{:S(2)}) copy-start(f32[32,4]{0,1:T(4,128)} %param.10) | copy-start | bytes 1540
